TPU v7x, 32 devices: a whole 2x2x4 slice. The times are simulated.
32 devices in a mesh: fs: 4 (over z), rep: 4 (over y, x), tp: 2 (over core).
Axes of the slice: x: 2, y: 2, z: 4, core: 2. Of those that a mesh axis runs over, the one named last changes fastest.
Arguments:
- saved_input: bfloat16 [5632, 2048], P(('fs', 'rep')), may hold values from -6 to 6
- query_cot: bfloat16 [5632, 1024], P(('fs', 'rep'), 'tp'), may hold values from -0.078125 to 0.078125
- attn_out: bfloat16 [5632, 1024], P(('fs', 'rep'), 'tp'), may hold values from -6 to 6
- out_cot: bfloat16 [5632, 2048], P(('fs', 'rep')), may hold values from -0.078125 to 0.078125
- query_basis: bfloat16 [2048, 512], P('fs'), may hold values from -0.25 to 0.25
- output_basis: bfloat16 [2048, 512], P('fs'), may hold values from -0.25 to 0.25
- query_weight: float32 [2048, 1024], P('fs', 'tp'), may hold values from -6 to 6
- output_weight: float32 [1024, 2048], P('tp', 'fs'), may hold values from -6 to 6
- query_moment: float32 [512, 1024], P('rep', 'tp'), may hold values from -52 to 52
- output_moment: float32 [1024, 512], P('tp', 'rep'), may hold values from -52 to 52
Outputs:
- query_step: float32 [2048, 1024], P('fs', 'tp')
- output_step: float32 [1024, 2048], P('tp', 'fs')
- query_new: float32 [2048, 1024], P('fs', 'tp')
- output_new: float32 [1024, 2048], P('tp', 'fs')
- query_copy: bfloat16 [2048, 1024], P('fs', 'tp')
- output_copy: bfloat16 [1024, 2048], P('tp', 'fs')
- query_moment_new: float32 [512, 1024], P('rep', 'tp')
- output_moment_new: float32 [1024, 512], P('tp', 'rep')
All inputs are finite; a program needn't handle non-finite values.
Results may differ from a plain program's by a relative error of at most 0.0029.
Values may be sent and summed in bfloat16 or wider, within the bound.
A program may use at most 64 MiB of HBM per device.

v0:
```python
import jax
import jax.numpy as jnp
from jax import lax
from jax.sharding import PartitionSpec as P

BETA = 0.8
RATE = 0.2
EPS = 1e-06


def on_device(
    saved_input,
    query_cot,
    attn_out,
    out_cot,
    query_basis,
    output_basis,
    query_weight,
    output_weight,
    query_moment,
    output_moment,
):
    rank = query_basis.shape[1]
    grad_rows = lax.psum_scatter(
        jnp.dot(saved_input.T, query_cot, preferred_element_type=jnp.float32),
        "fs",
        scatter_dimension=0,
        tiled=True,
    )
    query_part = jnp.dot(
        query_basis.astype(jnp.float32).T, grad_rows, precision=lax.Precision.HIGHEST
    )
    cot_proj = jnp.dot(
        out_cot,
        lax.all_gather(output_basis, "fs", axis=0, tiled=True),
        preferred_element_type=jnp.float32,
    )
    output_part = jnp.dot(attn_out.astype(jnp.float32).T, cot_proj, precision=lax.Precision.HIGHEST)
    reps = lax.axis_size("rep")
    share = rank // reps
    query_terms, output_terms = (
        lax.all_to_all(
            query_part.astype(jnp.bfloat16), "rep", split_axis=0, concat_axis=0, tiled=True
        ).astype(query_part.dtype),
        lax.all_to_all(
            output_part.T.astype(jnp.bfloat16), "rep", split_axis=0, concat_axis=0, tiled=True
        ).astype(jnp.float32),
    )
    width = query_part.shape[1]
    query_local = jnp.sum(query_terms.reshape(reps, share, width), axis=0)
    output_local = jnp.sum(output_terms.reshape(reps, share, width), axis=0)
    query_share, output_flip = lax.psum((query_local, output_local), "fs")
    output_share = output_flip.T
    query_moment_new = BETA * query_moment + (1.0 - BETA) * query_share
    output_moment_new = BETA * output_moment + (1.0 - BETA) * output_share
    query_squares, output_squares = lax.psum(
        (
            jnp.sum(query_moment_new * query_moment_new),
            jnp.sum(output_moment_new * output_moment_new),
        ),
        ("rep", "tp"),
    )
    entries = rank * query_moment.shape[1] * lax.axis_size("tp")
    query_dir = (query_moment_new * lax.rsqrt(query_squares / entries + EPS)).astype(jnp.bfloat16)
    output_dir = (output_moment_new * lax.rsqrt(output_squares / entries + EPS)).astype(
        jnp.bfloat16
    )
    query_full, output_full = (
        lax.all_gather(query_dir, "rep", axis=0, tiled=True),
        lax.all_gather(output_dir, "rep", axis=1, tiled=True),
    )
    query_step = jnp.dot(query_basis, query_full, preferred_element_type=jnp.float32)
    output_step = jnp.dot(output_full, output_basis.T, preferred_element_type=jnp.float32)
    query_new = query_weight - RATE * query_step
    output_new = output_weight - RATE * output_step
    return (
        query_step,
        output_step,
        query_new,
        output_new,
        query_new.astype(jnp.bfloat16),
        output_new.astype(jnp.bfloat16),
        query_moment_new,
        output_moment_new,
    )


def solution(mesh):
    placed = (
        P(("fs", "rep"), None),
        P(("fs", "rep"), "tp"),
        P(("fs", "rep"), "tp"),
        P(("fs", "rep"), None),
        P("fs", None),
        P("fs", None),
        P("fs", "tp"),
        P("tp", "fs"),
        P("rep", "tp"),
        P("tp", "rep"),
    )
    return jax.shard_map(
        on_device,
        mesh=mesh,
        in_specs=placed,
        out_specs=(
            P("fs", "tp"),
            P("tp", "fs"),
            P("fs", "tp"),
            P("tp", "fs"),
            P("fs", "tp"),
            P("tp", "fs"),
            P("rep", "tp"),
            P("tp", "rep"),
        ),
        check_vma=False,
    )
```

profile of v0, /device:TPU:0, one launch (start us, length us, event | category | flops | bytes accessed | tf_op | source)
XLA Modules:
  0.0 253.2 jit_solution(7196778270909197220)
XLA Ops:
  8.5 4.2 %fusion.2 = f32[2048,512]{1,0:T(8,128)} fusion(bf16[352,2048]{1,0:T(8,128)(2,1)S(1)} %copy-done, bf16[352,512]{1,0:T(8,128)(2,1)} %param.11), kind=kOutput, calls=%fused_computation.15 | convolution fusion | flops 738197504 | bytes 5996544 | tf_op jit(solution)/shard_map/dot_general | solution.py:25
  12.8 45.2 %all-gather.2.cloned.1.call-done = bf16[2048,512]{1,0:T(8,128)(2,1)} async-done(((bf16[512,512]{1,0:T(8,128)(2,1)}), bf16[2048,512]{1,0:T(8,128)(2,1)}) %all-gather.2.cloned.1.call-update) | async-done | bytes 2097168 | tf_op jit(solution)/shard_map/all_gather | solution.py:35
  58.0 2.9 %fusion.3 = f32[352,512]{1,0:T(8,128)S(1)} fusion(bf16[352,2048]{1,0:T(8,128)(2,1)} %param.13, bf16[2048,512]{1,0:T(8,128)(2,1)} %all-gather.2.cloned.1.call-done), kind=kOutput, calls=%fused_computation.16 | convolution fusion | flops 738197504 | bytes 4259840 | tf_op jit(solution)/shard_map/dot_general | solution.py:33
  60.9 1.8 convolution_convert_fusion
  62.8 3.7 %all-to-all-start.1 = ((bf16[4,128,512]{2,1,0:T(8,128)(2,1)}), bf16[4,128,512]{2,1,0:T(8,128)(2,1)S(1)}, u32[]{:S(2)}, u32[]{:S(2)}) async-start(bf16[4,128,512]{2,1,0:T(8,128)(2,1)} %bitcast.3), calls=%async_computation.2 | async-start | bytes 1048576 | tf_op jit(solution)/shard_map/all_to_all | solution.py:45
  66.4 69.5 %reduce-scatter.2.cloned.1.call-done = f32[512,512]{1,0:T(8,128)} async-done(((f32[2048,512]{1,0:T(8,128)}), f32[512,512]{1,0:T(8,128)}) %reduce-scatter.2.cloned.1.call-update) | async-done | bytes 1048592 | tf_op jit(solution)/shard_map/reduce_scatter | solution.py:24
  135.9 3.1 %convolution_convert_fusion.1 = bf16[512,512]{0,1:T(8,128)(2,1)} fusion(f32[512,512]{1,0:T(8,128)} %reduce-scatter.2.cloned.1.call-done, bf16[512,512]{1,0:T(8,128)(2,1)S(1)} %copy-done.4), kind=kOutput, calls=%fused_computation.2 | convolution fusion | flops 1610874880 | bytes 2097152 | tf_op jit(solution)/shard_map/dot_general | solution.py:30
  139.0 3.7 %all-to-all-start = ((bf16[4,128,512]{2,1,0:T(8,128)(2,1)}), bf16[4,128,512]{2,1,0:T(8,128)(2,1)S(1)}, u32[]{:S(2)}, u32[]{:S(2)}) async-start(bf16[4,128,512]{2,1,0:T(8,128)(2,1)} %bitcast.1), calls=%async_computation.1 | async-start | bytes 1048576 | tf_op jit(solution)/shard_map/all_to_all | solution.py:42
  143.4 7.0 %all-to-all-done = bf16[4,128,512]{2,1,0:T(8,128)(2,1)S(1)} async-done(((bf16[4,128,512]{2,1,0:T(8,128)(2,1)}), bf16[4,128,512]{2,1,0:T(8,128)(2,1)S(1)}, u32[]{:S(2)}, u32[]{:S(2)}) %all-to-all-start) | async-done | bytes 524320 | tf_op jit(solution)/shard_map/all_to_all | solution.py:42
  152.4 2.6 %copy.29 = f32[512,512]{0,1:T(8,128)} copy(f32[512,512]{1,0:T(8,128)} %param.16) | data formatting | bytes 2097152 | tf_op args[6]
  155.0 34.8 %all-reduce.4.cloned.1.call-done = (f32[128,512]{1,0:T(8,128)}, f32[128,512]{1,0:T(8,128)}) async-done(((f32[128,512]{1,0:T(8,128)}, f32[128,512]{1,0:T(8,128)}), (f32[128,512]{1,0:T(8,128)}, f32[128,512]{1,0:T(8,128)})) %all-reduce.4.cloned.1.call-update) | async-done | bytes 524304 | tf_op jit(solution)/shard_map/psum | solution.py:52
  189.8 1.6 multiply_reduce_fusion
  191.5 2.3 multiply_reduce_fusion.1
  193.8 13.3 %all-reduce = (f32[]{:T(128)}, f32[]{:T(128)}) all-reduce(f32[]{:T(128)} %get-tuple-element.34, f32[]{:T(128)} %get-tuple-element.32), channel_id=1, replica_groups=mesh['fs'=4,'rep'=4,'tp'=2] {'rep','tp'}, use_global_device_ids=true, to_apply=%region_4.0 | all-reduce | flops 2 | bytes 16 | tf_op jit(solution)/shard_map/psum | solution.py:56
  208.7 9.1 %all_gather.11 = bf16[512,512]{0,1:T(8,128)(2,1)S(1)} all-gather(bf16[512,128]{0,1:T(8,128)(2,1)S(1)} %multiply_convert_fusion), channel_id=1, replica_groups=mesh['fs'=4,'rep'=4,'tp'=2] {'rep'}, dimensions={1}, use_global_device_ids=true | all-gather | bytes 655360 | tf_op jit(solution)/shard_map/all_gather | solution.py:70
  217.8 1.5 fusion.4
  220.3 1.3 copy.30
  221.6 2.3 fusion
  223.8 1.3 copy.34
  225.2 2.1 copy.36
  229.0 10.2 %all_gather.9 = bf16[512,512]{1,0:T(8,128)(2,1)S(1)} all-gather(bf16[128,512]{1,0:T(8,128)(2,1)S(1)} %multiply_convert_fusion.1), channel_id=1, replica_groups=mesh['fs'=4,'rep'=4,'tp'=2] {'rep'}, dimensions={0}, use_global_device_ids=true | all-gather | bytes 655360 | tf_op jit(solution)/shard_map/all_gather | solution.py:69
  239.1 2.7 %fusion.1 = (bf16[512,512]{0,1:T(8,128)(2,1)}, f32[512,512]{0,1:T(8,128)S(1)}, f32[512,512]{0,1:T(8,128)}) fusion(f32[512,512]{0,1:T(8,128)S(1)} %copy-done.2, bf16[512,512]{1,0:T(8,128)(2,1)S(1)} %all_gather.9, bf16[512,512]{1,0:T(8,128)(2,1)} %param.14), kind=kOutput, calls=%fused_computation.14 | convolution fusion | flops 269221888 | bytes 4718592 | tf_op jit(solution)/shard_map/dot_general | solution.py:72
  241.8 2.5 copy.32
  244.4 1.3 copy.33
  (35 shorter events, 7.9 us)
Async XLA Ops:
  7.2 1.4 copy-start
  7.2 50.8 %all-gather.2.cloned.1.call-start = ((), (), s32[]{:S(2)}) async-start(), calls=%async_computation.4 | async-start | bytes 2621440 | tf_op jit(solution)/shard_map/all_gather | solution.py:35
  7.9 128.0 %reduce-scatter.2.cloned.1.call-start = ((), (), s32[]{:S(2)}) async-start(), calls=%async_computation.3 | async-start | bytes 5242880 | tf_op jit(solution)/shard_map/reduce_scatter | solution.py:24
  12.8 48.1 %copy-start.7 = (bf16[352,512]{1,0:T(8,128)(2,1)S(1)}, bf16[352,512]{1,0:T(8,128)(2,1)}, u32[]{:S(2)}) copy-start(bf16[352,512]{1,0:T(8,128)(2,1)} %param.12) | copy-start | bytes 1081348
  60.9 75.0 %copy-start.4 = (bf16[512,512]{1,0:T(8,128)(2,1)S(1)}, bf16[512,512]{1,0:T(8,128)(2,1)}, u32[]{:S(2)}) copy-start(bf16[512,512]{1,0:T(8,128)(2,1)} %param.14) | copy-start | bytes 1572868
  62.8 76.2 %all-to-all-start.1 = ((bf16[4,128,512]{2,1,0:T(8,128)(2,1)}), bf16[4,128,512]{2,1,0:T(8,128)(2,1)S(1)}, u32[]{:S(2)}, u32[]{:S(2)}) async-start(bf16[4,128,512]{2,1,0:T(8,128)(2,1)} %bitcast.3), calls=%async_computation.2 | async-start | bytes 1048576 | tf_op jit(solution)/shard_map/all_to_all | solution.py:45
  139.0 11.4 %all-to-all-start = ((bf16[4,128,512]{2,1,0:T(8,128)(2,1)}), bf16[4,128,512]{2,1,0:T(8,128)(2,1)S(1)}, u32[]{:S(2)}, u32[]{:S(2)}) async-start(bf16[4,128,512]{2,1,0:T(8,128)(2,1)} %bitcast.1), calls=%async_computation.1 | async-start | bytes 1048576 | tf_op jit(solution)/shard_map/all_to_all | solution.py:42
  142.6 9.4 %copy-start.5 = (f32[512,512]{1,0:T(8,128)S(1)}, f32[512,512]{1,0:T(8,128)}, u32[]{:S(2)}) copy-start(f32[512,512]{1,0:T(8,128)} %param.17) | copy-start | bytes 3145732
  142.6 47.2 %all-reduce.4.cloned.1.call-start = ((), (), s32[]{:S(2)}) async-start(), calls=%async_computation.5 | async-start | bytes 1048576 | tf_op jit(solution)/shard_map/psum | solution.py:52
  143.4 7.8 %copy-start.8 = (f32[512,128]{1,0:T(8,128)S(1)}, f32[512,128]{1,0:T(8,128)}, u32[]{:S(2)}) copy-start(f32[512,128]{1,0:T(8,128)} %param.19) | copy-start | bytes 786436
  152.4 37.4 %copy-start.6 = (f32[512,128]{0,1:T(8,128)S(1)}, f32[512,128]{0,1:T(8,128)}, u32[]{:S(2)}) copy-start(f32[512,128]{0,1:T(8,128)} %copy.28) | copy-start | bytes 786436
  152.4 39.1 %copy-start.9 = (f32[128,512]{1,0:T(8,128)S(1)}, f32[128,512]{1,0:T(8,128)}, u32[]{:S(2)}) copy-start(f32[128,512]{1,0:T(8,128)} %param.18) | copy-start | bytes 786436
  219.3 1.0 copy-start.1
  225.2 14.0 %copy-start.2 = (f32[512,512]{0,1:T(8,128)S(1)}, f32[512,512]{0,1:T(8,128)}, u32[]{:S(2)}) copy-start(f32[512,512]{0,1:T(8,128)} %copy.29) | copy-start | bytes 3145732
  244.4 1.3 copy-start.3
Sparse Core Ops, SparseCore 0:
  9.6 48.3 all-gather.1
  60.3 75.5 reduce-scatter.1
  151.3 38.4 all-reduce.3
where the time goes:
time: 254 us; the launch traced here: 253 us
  waiting for transfers between devices  157 us (62%)
  blocking collectives  32.6 us (13%)
  matrix products  16.3 us (6%)
  local copies, waits for them, and re-layouts  15.8 us (6%)
  between operations  15.2 us (6%)
  other arithmetic  8.72 us (3%)
  starting transfers between devices  7.38 us (3%)
    reduce_scatter x1, waiting for transfers between devices, on_device(): lax.psum_scatter(jnp.dot(saved_input.T, query_cot, preferred_element_type...  69.5 us
    all_gather x1, waiting for transfers between devices, on_device(): lax.all_gather(output_basis, 'fs', axis=0, tiled=True)  45.2 us
    psum x1, waiting for transfers between devices, on_device(): query_share, output_flip = lax.psum((query_local, output_local), 'fs')  34.8 us
    unnamed x29, local copies, waits for them, and re-layouts  14.5 us
    psum x1, blocking collectives, on_device(): lax.psum((jnp.sum(query_moment_new * query_moment_new), jnp.sum(output_mo...  13.3 us
    all_gather x1, blocking collectives, on_device(): lax.all_gather(query_dir, 'rep', axis=0, tiled=True)  10.2 us
    all_gather x1, blocking collectives, on_device(): lax.all_gather(output_dir, 'rep', axis=1, tiled=True)  9.09 us
    all_to_all x1, waiting for transfers between devices, on_device(): lax.all_to_all(query_part.astype(jnp.bfloat16), 'rep', split_axis=0, conc...  7.01 us
  transfers between devices with their start and end apart: 5, of which 4 were waited for; matrix products, arithmetic and copies ran while one was open for 7% of the time, Pallas kernels for 0%

commit v1 on v0

--- a/solution.py
+++ b/solution.py
@@ -1,6 +1,10 @@
+import functools
+
 import jax
 import jax.numpy as jnp
 from jax import lax
+from jax.experimental import pallas as pl
+from jax.experimental.pallas import tpu as pltpu
 from jax.sharding import PartitionSpec as P
 
 BETA = 0.8
@@ -85,7 +89,292 @@
     )
 
 
+MESH = pl.DeviceIdType.MESH
+
+
+def exchange_kernel(
+    entries,
+    si_hbm, oc_hbm, qc_hbm, ao_hbm, qb_hbm, ob_hbm, mq_hbm, mo_hbm,
+    full_out, mom_out,
+    act, cot, base, mq, mo, gath, xb, pb, t1, t2, mom, nrm, full,
+    load_sem, store_sem, az_s, az_r, aw_s, aw_r, xc_s, xc_r,
+    b1_s, b1_r, b2_s, b2_r, n_s, n_r, d_s, d_r,
+):
+    f, r, t = lax.axis_index("fs"), lax.axis_index("rep"), lax.axis_index("tp")
+    y, x = r // 2, r % 2
+    ot = 1 - t
+    fpeer = [(f + d) % 4 for d in (1, 3, 2)]
+    fsrc = [(f + 4 - d) % 4 for d in (1, 3, 2)]
+    rpeer = [2 * y + (1 - x), 2 * (1 - y) + x, 3 - r]
+    depth, rank = base.shape[1], base.shape[2]
+    hd, hr = depth // 2, rank // 2
+    share = rank // 4
+
+    loads = []
+    for k, (src, dst) in enumerate((
+        (qb_hbm, base.at[0]), (ob_hbm, base.at[1]), (si_hbm, act.at[0]), (oc_hbm, act.at[1]),
+        (qc_hbm, cot.at[0]), (ao_hbm, cot.at[1]), (mq_hbm, mq), (mo_hbm, mo),
+    )):
+        c = pltpu.make_async_copy(src, dst, load_sem.at[k])
+        c.start()
+        loads.append(c)
+
+    barrier = pltpu.get_barrier_semaphore()
+    for g in fpeer:
+        pl.semaphore_signal(barrier, inc=1, device_id=(g, r, t), device_id_type=MESH)
+    for q in rpeer:
+        for s in (t, ot):
+            pl.semaphore_signal(barrier, inc=1, device_id=(f, q, s), device_id_type=MESH)
+    pl.semaphore_signal(barrier, inc=1, device_id=(f, r, ot), device_id_type=MESH)
+    pl.semaphore_wait(barrier, 10)
+
+    def remote(src, dst, ss, rs, dev):
+        return pltpu.make_async_remote_copy(
+            src_ref=src, dst_ref=dst, send_sem=ss, recv_sem=rs, device_id=dev, device_id_type=MESH
+        )
+
+    half = (x, y)
+    near = (rpeer[0], rpeer[1])
+    cols = pl.ds(pl.multiple_of(t * hr, hr), hr)
+    sends = []
+    zs = [[], []]
+    for p in range(2):
+        loads[p].wait()
+        rows = pl.ds(pl.multiple_of(half[p] * hd, hd), hd)
+        for k in range(3):
+            c = remote(
+                base.at[p, rows, cols], gath.at[p, f, rows, :],
+                az_s.at[p, k], az_r.at[p, k], (fpeer[k], r, t),
+            )
+            c.start()
+            zs[p].append(c)
+    ws = [[], []]
+    for k in range(3):
+        for p in range(2):
+            rows = pl.ds(pl.multiple_of(half[p] * hd, hd), hd)
+            zs[p][k].wait_recv()
+            c = remote(
+                gath.at[p, fsrc[k], rows, :], gath.at[p, fsrc[k], rows, :],
+                aw_s.at[p, k], aw_r.at[p, k], (f, near[p], t),
+            )
+            c.start()
+            ws[p].append(c)
+
+    def slab(p, g, weights):
+        return jnp.dot(
+            act[p, :, pl.ds(pl.multiple_of(g * depth, depth), depth)], weights,
+            preferred_element_type=jnp.float32,
+        )
+
+    loads[2].wait()
+    loads[3].wait()
+    accs = [slab(p, f, base[p, :, cols]) for p in range(2)]
+    xs = []
+    for p in range(2):
+        acc = accs[p]
+        for k in range(3):
+            ws[p][k].wait_recv()
+            acc = acc + slab(p, fsrc[k], gath[p, fsrc[k]])
+        xb[p, t] = acc.astype(jnp.bfloat16)
+        c = remote(xb.at[p, t], xb.at[p, t], xc_s.at[p], xc_r.at[p], (f, r, ot))
+        c.start()
+        xs.append(c)
+
+    b1 = [[], []]
+    for p in range(2):
+        loads[4 + p].wait()
+        xs[p].wait_recv()
+        for j in range(2):
+            part = lax.dot_general(
+                xb[p, j], cot[p], (((0,), (0,)), ((), ())), preferred_element_type=jnp.float32
+            )
+            for i in range(2):
+                pb[p, 2 * j + i] = part[i * share : (i + 1) * share].astype(jnp.bfloat16)
+        for k in (2, 0, 1):
+            c = remote(
+                pb.at[p, rpeer[k]], t1.at[p, k], b1_s.at[p, k], b1_r.at[p, k], (f, rpeer[k], t)
+            )
+            c.start()
+            b1[p].append(c)
+
+    b2 = [[], []]
+    for p in range(2):
+        for c in b1[p]:
+            c.wait_recv()
+        total = pb[p, r].astype(jnp.float32)
+        for k in range(3):
+            total = total + t1[p, k].astype(jnp.float32)
+        t2[p, f] = total.astype(jnp.bfloat16)
+        for k in (2, 0, 1):
+            c = remote(
+                t2.at[p, f], t2.at[p, f], b2_s.at[p, k], b2_r.at[p, k], (fpeer[k], r, t)
+            )
+            c.start()
+            b2[p].append(c)
+
+    loads[6].wait()
+    loads[7].wait()
+    others = [(q, s) for q in rpeer for s in (t, ot)] + [(r, ot)]
+    ns = [[], []]
+    me = 2 * r + t
+    for p in range(2):
+        old = mq[...] if p == 0 else mo[...].T
+        for c in b2[p]:
+            c.wait_recv()
+        total = t2[p, 0].astype(jnp.float32)
+        for g in range(1, 4):
+            total = total + t2[p, g].astype(jnp.float32)
+        new = BETA * old + (1.0 - BETA) * total
+        mom[p] = new
+        sq = new * new
+        lanes = sq[:, :128]
+        for k in range(1, sq.shape[1] // 128):
+            lanes = lanes + sq[:, k * 128 : (k + 1) * 128]
+        acc = lanes[:8]
+        for k in range(1, share // 8):
+            acc = acc + lanes[k * 8 : (k + 1) * 8]
+        nrm[p, me] = acc
+        for k, (q, s) in enumerate(others):
+            c = remote(nrm.at[p, me], nrm.at[p, me], n_s.at[p, k], n_r.at[p, k], (f, q, s))
+            c.start()
+            ns[p].append(c)
+
+    stores = []
+    ds = [[], []]
+    for p in range(2):
+        c = pltpu.make_async_copy(mom.at[p], mom_out.at[p], store_sem.at[p])
+        c.start()
+        stores.append(c)
+        for c in ns[p]:
+            c.wait_recv()
+        acc = nrm[p, 0]
+        for k in range(1, 8):
+            acc = acc + nrm[p, k]
+        squares = jnp.sum(jnp.sum(acc, axis=0, keepdims=True), axis=1, keepdims=True)
+        full[p, r] = (mom[p] * lax.rsqrt(squares / entries + EPS)).astype(jnp.bfloat16)
+        for k in (2, 0, 1):
+            c = remote(
+                full.at[p, r], full.at[p, r], d_s.at[p, k], d_r.at[p, k], (f, rpeer[k], t)
+            )
+            c.start()
+            ds[p].append(c)
+    for p in range(2):
+        for c in ds[p]:
+            c.wait_recv()
+        c = pltpu.make_async_copy(full.at[p], full_out.at[p], store_sem.at[2 + p])
+        c.start()
+        stores.append(c)
+    for group in (zs, ws, b1, b2, ns, ds, [xs]):
+        for part in group:
+            for c in part:
+                c.wait_send()
+    for c in stores:
+        c.wait()
+
+
+def finish_kernel(
+    qb, ob, fq, fo, qw, ow, mq, mo, qs_o, os_o, qn_o, on_o, qc_o, oc_o, mq_o, mo_o
+):
+    step = jnp.dot(qb[...], fq[0], preferred_element_type=jnp.float32)
+    new = qw[...] - RATE * step
+    qs_o[...] = step
+    qn_o[...] = new
+    qc_o[...] = new.astype(jnp.bfloat16)
+    step = lax.dot_general(
+        fo[0].T, ob[...], (((1,), (1,)), ((), ())), preferred_element_type=jnp.float32
+    )
+    new = ow[...] - RATE * step
+    os_o[...] = step
+    on_o[...] = new
+    oc_o[...] = new.astype(jnp.bfloat16)
+    mq_o[...] = mq[0]
+    mo_o[...] = mo[0].T
+
+
+def on_device_fast(
+    saved_input, query_cot, attn_out, out_cot, query_basis, output_basis,
+    query_weight, output_weight, query_moment, output_moment,
+):
+    tokens, depth_all = saved_input.shape
+    width = query_cot.shape[1]
+    depth, rank = query_basis.shape
+    share = rank // 4
+    entries = rank * width * lax.axis_size("tp")
+    bf, f32 = jnp.bfloat16, jnp.float32
+    any_spec = pl.BlockSpec(memory_space=pl.ANY)
+    dma = pltpu.SemaphoreType.DMA
+    full, mom = pl.pallas_call(
+        functools.partial(exchange_kernel, entries),
+        out_shape=(
+            jax.ShapeDtypeStruct((2, 4, share, width), bf),
+            jax.ShapeDtypeStruct((2, share, width), f32),
+        ),
+        in_specs=[any_spec] * 8,
+        out_specs=(any_spec, any_spec),
+        scratch_shapes=[
+            pltpu.VMEM((2, tokens, depth_all), bf),
+            pltpu.VMEM((2, tokens, width), bf),
+            pltpu.VMEM((2, depth, rank), bf),
+            pltpu.VMEM((share, width), f32),
+            pltpu.VMEM((width, share), f32),
+            pltpu.VMEM((2, 4, depth, rank // 2), bf),
+            pltpu.VMEM((2, 2, tokens, rank // 2), bf),
+            pltpu.VMEM((2, 4, share, width), bf),
+            pltpu.VMEM((2, 3, share, width), bf),
+            pltpu.VMEM((2, 4, share, width), bf),
+            pltpu.VMEM((2, share, width), f32),
+            pltpu.VMEM((2, 8, 8, 128), f32),
+            pltpu.VMEM((2, 4, share, width), bf),
+            dma((8,)), dma((4,)),
+            dma((2, 3)), dma((2, 3)), dma((2, 3)), dma((2, 3)),
+            dma((2,)), dma((2,)),
+            dma((2, 3)), dma((2, 3)), dma((2, 3)), dma((2, 3)),
+            dma((2, 7)), dma((2, 7)), dma((2, 3)), dma((2, 3)),
+        ],
+        compiler_params=pltpu.CompilerParams(
+            collective_id=0, has_side_effects=True, vmem_limit_bytes=60 * 2**20
+        ),
+    )(
+        saved_input, out_cot, query_cot, attn_out, query_basis, output_basis,
+        query_moment, output_moment,
+    )
+    full = full.reshape(2, rank, width)
+    n = 4
+    rows = pl.BlockSpec((depth // n, rank), lambda i: (i, 0))
+    whole = pl.BlockSpec((depth, rank), lambda i: (0, 0))
+    wq = pl.BlockSpec((depth // n, width), lambda i: (i, 0))
+    wo = pl.BlockSpec((width // n, depth), lambda i: (i, 0))
+    mq = pl.BlockSpec((share // n, width), lambda i: (i, 0))
+    mo = pl.BlockSpec((width // n, share), lambda i: (i, 0))
+    sq, so = query_weight.shape, output_weight.shape
+    return pl.pallas_call(
+        finish_kernel,
+        grid=(n,),
+        out_shape=tuple(
+            jax.ShapeDtypeStruct(s, d)
+            for s, d in (
+                (sq, f32), (so, f32), (sq, f32), (so, f32), (sq, bf), (so, bf),
+                (query_moment.shape, f32), (output_moment.shape, f32),
+            )
+        ),
+        in_specs=[
+            rows, whole,
+            pl.BlockSpec((1, rank, width), lambda i: (0, 0, 0)),
+            pl.BlockSpec((1, rank, width // n), lambda i: (1, 0, i)),
+            wq, wo,
+            pl.BlockSpec((1, share // n, width), lambda i: (0, i, 0)),
+            pl.BlockSpec((1, share, width // n), lambda i: (1, 0, i)),
+        ],
+        out_specs=(wq, wo, wq, wo, wq, wo, mq, mo),
+        cost_estimate=pl.CostEstimate(
+            flops=4 * depth * rank * width, bytes_accessed=20 * depth * width, transcendentals=0
+        ),
+    )(query_basis, output_basis, full, full, query_weight, output_weight, mom, mom)
+
+
 def solution(mesh):
+    small = dict(mesh.shape) == {"fs": 4, "rep": 4, "tp": 2}
+    body = on_device_fast if small else on_device
     placed = (
         P(("fs", "rep"), None),
         P(("fs", "rep"), "tp"),
@@ -99,7 +388,7 @@
         P("tp", "rep"),
     )
     return jax.shard_map(
-        on_device,
+        body,
         mesh=mesh,
         in_specs=placed,
         out_specs=(

time: 254 us -> 86.1 us (0.34)
  the two profiles are of different devices: /device:TPU:0 before, /device:TPU:10 now
where the time goes in v1:
time: 86.1 us; the launch traced here: 85.9 us
  Pallas kernels  85.2 us (99%)
    pallas_call x1, Pallas kernels, on_device_fast(): pl.pallas_call(functools.partial(exchange_kernel, entries), out_shape=(ja...  79.2 us
    pallas_call x1, Pallas kernels, on_device_fast(): pl.pallas_call(finish_kernel, grid=(n,), out_shape=tuple((jax.ShapeDtypeS...  5.97 us

profile of v1, /device:TPU:10, one launch (start us, length us, event | category | flops | bytes accessed | tf_op | source)
XLA Modules:
  0.0 85.9 jit_solution(7519796344708920239)
XLA Ops:
  0.6 79.2 %shard_map.161 = (bf16[2,4,128,512]{3,2,1,0:T(8,128)(2,1)}, f32[2,128,512]{2,1,0:T(8,128)}) custom-call(bf16[352,2048]{1,0:T(8,128)(2,1)} %si_hbm.1, bf16[352,2048]{1,0:T(8,128)(2,1)} %oc_hbm.1, bf16[352,512]{1,0:T(8,128)(2,1)} %qc_hbm.1, bf16[352,512]{1,0:T(8,128)(2,1)} %ao_hbm.1, bf16[512,512]{1,0:T(8,128)(2,1)} %qb.1, bf16[512,512]{1,0:T(8,128)(2,1)} %ob.1, ...), custom_call_target="tpu_custom_call" | custom-call | tf_op jit(solution)/shard_map/pallas_call | solution.py:306
  79.9 6.0 %shard_map.162 = (f32[512,512]{1,0:T(8,128)}, f32[512,512]{1,0:T(8,128)}, f32[512,512]{1,0:T(8,128)}, f32[512,512]{1,0:T(8,128)}, bf16[512,512]{1,0:T(8,128)(2,1...) custom-call(bf16[512,512]{1,0:T(8,128)(2,1)} %qb.1, bf16[512,512]{1,0:T(8,128)(2,1)} %ob.1, ...), custom_call_target="tpu_custom_call" | custom-call | flops 536870912 | bytes 5242880 | tf_op jit(solution)/shard_map/pallas_call | solution.py:350

commit v2 on v1

--- a/solution.py
+++ b/solution.py
@@ -96,9 +96,9 @@
     entries,
     si_hbm, oc_hbm, qc_hbm, ao_hbm, qb_hbm, ob_hbm, mq_hbm, mo_hbm,
     full_out, mom_out,
-    act, cot, base, mq, mo, gath, xb, pb, t1, t2, mom, nrm, full,
+    act, cot, base, mq, mo, gath, xb, pb, t1, sb, t2, ag, mom, nrm, full,
     load_sem, store_sem, az_s, az_r, aw_s, aw_r, xc_s, xc_r,
-    b1_s, b1_r, b2_s, b2_r, n_s, n_r, d_s, d_r,
+    b1_s, b1_r, b2_s, b2_r, g_s, g_r, n_s, n_r, d_s, d_r,
 ):
     f, r, t = lax.axis_index("fs"), lax.axis_index("rep"), lax.axis_index("tp")
     y, x = r // 2, r % 2
@@ -133,97 +133,141 @@
             src_ref=src, dst_ref=dst, send_sem=ss, recv_sem=rs, device_id=dev, device_id_type=MESH
         )
 
-    half = (x, y)
-    near = (rpeer[0], rpeer[1])
+    h = x * (1 - t) + y * t
+    near = rpeer[0] * (1 - t) + rpeer[1] * t
+    rows = pl.ds(pl.multiple_of(h * hd, hd), hd)
     cols = pl.ds(pl.multiple_of(t * hr, hr), hr)
-    sends = []
-    zs = [[], []]
-    for p in range(2):
+    last = 3
+
+    def line(p, way, s, arrive=False):
+        step = -1 if way == 0 else 1
+        slab = f + step * s + (step if arrive else 0)
+        dst = gath.at[p, slab, rows, :]
+        src = base.at[p, rows, cols] if s == 0 and not arrive else dst
+        dev = f + step if arrive else f - step
+        return remote(src, dst, az_s.at[p, way, s], az_r.at[p, way, s], (dev, r, t))
+
+    def sends_line(way, s):
+        return (f >= s) & (f < last) if way == 0 else (f + s <= last) & (f > 0)
+
+    def gets_line(way, s):
+        return f >= s + 1 if way == 0 else f + s + 1 <= last
+
+    def share_slab(p, slab):
+        return remote(
+            gath.at[p, slab, rows, :], gath.at[p, slab, rows, :],
+            aw_s.at[p, slab], aw_r.at[p, slab], (f, near, t),
+        )
+
+    def got_slab(p, slab):
+        orow = pl.ds(pl.multiple_of((1 - h) * hd, hd), hd)
+        return remote(
+            gath.at[p, slab, orow, :], gath.at[p, slab, orow, :],
+            aw_s.at[p, slab], aw_r.at[p, slab], (f, near, t),
+        )
+
+    def open_line(p):
         loads[p].wait()
-        rows = pl.ds(pl.multiple_of(half[p] * hd, hd), hd)
-        for k in range(3):
-            c = remote(
-                base.at[p, rows, cols], gath.at[p, f, rows, :],
-                az_s.at[p, k], az_r.at[p, k], (fpeer[k], r, t),
-            )
-            c.start()
-            zs[p].append(c)
-    ws = [[], []]
-    for k in range(3):
-        for p in range(2):
-            rows = pl.ds(pl.multiple_of(half[p] * hd, hd), hd)
-            zs[p][k].wait_recv()
-            c = remote(
-                gath.at[p, fsrc[k], rows, :], gath.at[p, fsrc[k], rows, :],
-                aw_s.at[p, k], aw_r.at[p, k], (f, near[p], t),
-            )
-            c.start()
-            ws[p].append(c)
-
-    def slab(p, g, weights):
+        for way in range(2):
+            @pl.when(sends_line(way, 0))
+            def _():
+                line(p, way, 0).start()
+
+    def run_line(s, p):
+        for way in range(2):
+            @pl.when(gets_line(way, s))
+            def _():
+                line(p, way, s, True).wait_recv()
+                slab = f - 1 - s if way == 0 else f + 1 + s
+                share_slab(p, slab).start()
+            if s < 2:
+                @pl.when(sends_line(way, s + 1))
+                def _():
+                    line(p, way, s + 1).start()
+
+    def slab_dot(p, g, weights):
         return jnp.dot(
             act[p, :, pl.ds(pl.multiple_of(g * depth, depth), depth)], weights,
             preferred_element_type=jnp.float32,
         )
 
-    loads[2].wait()
-    loads[3].wait()
-    accs = [slab(p, f, base[p, :, cols]) for p in range(2)]
-    xs = []
-    for p in range(2):
-        acc = accs[p]
-        for k in range(3):
-            ws[p][k].wait_recv()
-            acc = acc + slab(p, fsrc[k], gath[p, fsrc[k]])
+    def project(p, acc):
+        for g in fsrc:
+            got_slab(p, g).wait_recv()
+            acc = acc + slab_dot(p, g, gath[p, g])
         xb[p, t] = acc.astype(jnp.bfloat16)
         c = remote(xb.at[p, t], xb.at[p, t], xc_s.at[p], xc_r.at[p], (f, r, ot))
         c.start()
-        xs.append(c)
-
-    b1 = [[], []]
-    for p in range(2):
+        return c
+
+    def got_half(p):
+        return remote(xb.at[p, ot], xb.at[p, ot], xc_s.at[p], xc_r.at[p], (f, r, ot))
+
+    def scatter_reps(p):
         loads[4 + p].wait()
-        xs[p].wait_recv()
+        got_half(p).wait_recv()
         for j in range(2):
             part = lax.dot_general(
                 xb[p, j], cot[p], (((0,), (0,)), ((), ())), preferred_element_type=jnp.float32
             )
             for i in range(2):
                 pb[p, 2 * j + i] = part[i * share : (i + 1) * share].astype(jnp.bfloat16)
+        out = []
         for k in (2, 0, 1):
             c = remote(
                 pb.at[p, rpeer[k]], t1.at[p, k], b1_s.at[p, k], b1_r.at[p, k], (f, rpeer[k], t)
             )
             c.start()
-            b1[p].append(c)
-
-    b2 = [[], []]
-    for p in range(2):
-        for c in b1[p]:
+            out.append(c)
+        return out
+
+    piece = share // 4
+
+    def scatter_tokens(p, arrivals):
+        for c in arrivals:
             c.wait_recv()
         total = pb[p, r].astype(jnp.float32)
         for k in range(3):
             total = total + t1[p, k].astype(jnp.float32)
-        t2[p, f] = total.astype(jnp.bfloat16)
+        for g in range(4):
+            sb[p, g] = total[g * piece : (g + 1) * piece].astype(jnp.bfloat16)
+        out = []
         for k in (2, 0, 1):
             c = remote(
-                t2.at[p, f], t2.at[p, f], b2_s.at[p, k], b2_r.at[p, k], (fpeer[k], r, t)
+                sb.at[p, fpeer[k]], t2.at[p, k], b2_s.at[p, k], b2_r.at[p, k], (fpeer[k], r, t)
             )
             c.start()
-            b2[p].append(c)
-
-    loads[6].wait()
-    loads[7].wait()
+            out.append(c)
+        return out
+
+    def gather_sums(p, arrivals):
+        for c in arrivals:
+            c.wait_recv()
+        total = sb[p, f].astype(jnp.float32)
+        for k in range(3):
+            total = total + t2[p, k].astype(jnp.float32)
+        ag[p, f] = total.astype(jnp.bfloat16)
+        out = []
+        for k in (2, 0, 1):
+            c = remote(
+                ag.at[p, f], ag.at[p, f], g_s.at[p, k], g_r.at[p, k], (fpeer[k], r, t)
+            )
+            c.start()
+            out.append(c)
+        return out
+
+    def got_sums(p, k):
+        src = fsrc[k]
+        return remote(ag.at[p, src], ag.at[p, src], g_s.at[p, k], g_r.at[p, k], (src, r, t))
+
     others = [(q, s) for q in rpeer for s in (t, ot)] + [(r, ot)]
-    ns = [[], []]
     me = 2 * r + t
-    for p in range(2):
+
+    def update_moment(p):
         old = mq[...] if p == 0 else mo[...].T
-        for c in b2[p]:
-            c.wait_recv()
-        total = t2[p, 0].astype(jnp.float32)
-        for g in range(1, 4):
-            total = total + t2[p, g].astype(jnp.float32)
+        for k in range(3):
+            got_sums(p, k).wait_recv()
+        total = ag[p].astype(jnp.float32).reshape(old.shape)
         new = BETA * old + (1.0 - BETA) * total
         mom[p] = new
         sq = new * new
@@ -234,40 +278,80 @@
         for k in range(1, share // 8):
             acc = acc + lanes[k * 8 : (k + 1) * 8]
         nrm[p, me] = acc
+        out = []
         for k, (q, s) in enumerate(others):
             c = remote(nrm.at[p, me], nrm.at[p, me], n_s.at[p, k], n_r.at[p, k], (f, q, s))
             c.start()
-            ns[p].append(c)
-
-    stores = []
-    ds = [[], []]
-    for p in range(2):
-        c = pltpu.make_async_copy(mom.at[p], mom_out.at[p], store_sem.at[p])
-        c.start()
-        stores.append(c)
-        for c in ns[p]:
-            c.wait_recv()
+            out.append(c)
+        return out
+
+    def gather_dirs(p):
+        for k, (q, s) in enumerate(others):
+            slot = 2 * q + s
+            remote(
+                nrm.at[p, slot], nrm.at[p, slot], n_s.at[p, k], n_r.at[p, k], (f, q, s)
+            ).wait_recv()
         acc = nrm[p, 0]
         for k in range(1, 8):
             acc = acc + nrm[p, k]
         squares = jnp.sum(jnp.sum(acc, axis=0, keepdims=True), axis=1, keepdims=True)
         full[p, r] = (mom[p] * lax.rsqrt(squares / entries + EPS)).astype(jnp.bfloat16)
+        out = []
         for k in (2, 0, 1):
             c = remote(
                 full.at[p, r], full.at[p, r], d_s.at[p, k], d_r.at[p, k], (f, rpeer[k], t)
             )
             c.start()
-            ds[p].append(c)
+            out.append(c)
+        return out
+
+    open_line(0)
+    open_line(1)
+    loads[2].wait()
+    loads[3].wait()
+    accs = [slab_dot(p, f, base[p, :, cols]) for p in range(2)]
+    for s in range(3):
+        run_line(s, 0)
+        run_line(s, 1)
+    x0 = project(0, accs[0])
+    b1q = scatter_reps(0)
+    x1 = project(1, accs[1])
+    b2q = scatter_tokens(0, b1q)
+    b1o = scatter_reps(1)
+    gq = gather_sums(0, b2q)
+    b2o = scatter_tokens(1, b1o)
+    loads[6].wait()
+    nq = update_moment(0)
+    go = gather_sums(1, b2o)
+    dq = gather_dirs(0)
+    loads[7].wait()
+    no = update_moment(1)
+    stores = []
     for p in range(2):
-        for c in ds[p]:
-            c.wait_recv()
+        c = pltpu.make_async_copy(mom.at[p], mom_out.at[p], store_sem.at[p])
+        c.start()
+        stores.append(c)
+    do = gather_dirs(1)
+    for p in range(2):
+        for k in range(3):
+            remote(
+                full.at[p, rpeer[k]], full.at[p, rpeer[k]],
+                d_s.at[p, k], d_r.at[p, k], (f, rpeer[k], t),
+            ).wait_recv()
         c = pltpu.make_async_copy(full.at[p], full_out.at[p], store_sem.at[2 + p])
         c.start()
         stores.append(c)
-    for group in (zs, ws, b1, b2, ns, ds, [xs]):
-        for part in group:
-            for c in part:
-                c.wait_send()
+    for p in range(2):
+        for s in range(3):
+            for way in range(2):
+                @pl.when(sends_line(way, s))
+                def _():
+                    line(p, way, s).wait_send()
+        for g in fsrc:
+            share_slab(p, g).wait_send()
+    for group in (b1q, b1o, b2q, b2o, gq, go, nq, no, dq, do, [x0, x1]):
+        for c in group:
+            c.wait_send()
     for c in stores:
         c.wait()
 
@@ -321,14 +405,16 @@
             pltpu.VMEM((2, 2, tokens, rank // 2), bf),
             pltpu.VMEM((2, 4, share, width), bf),
             pltpu.VMEM((2, 3, share, width), bf),
-            pltpu.VMEM((2, 4, share, width), bf),
+            pltpu.VMEM((2, 4, share // 4, width), bf),
+            pltpu.VMEM((2, 3, share // 4, width), bf),
+            pltpu.VMEM((2, 4, share // 4, width), bf),
             pltpu.VMEM((2, share, width), f32),
             pltpu.VMEM((2, 8, 8, 128), f32),
             pltpu.VMEM((2, 4, share, width), bf),
             dma((8,)), dma((4,)),
-            dma((2, 3)), dma((2, 3)), dma((2, 3)), dma((2, 3)),
+            dma((2, 2, 3)), dma((2, 2, 3)), dma((2, 4)), dma((2, 4)),
             dma((2,)), dma((2,)),
-            dma((2, 3)), dma((2, 3)), dma((2, 3)), dma((2, 3)),
+            dma((2, 3)), dma((2, 3)), dma((2, 3)), dma((2, 3)), dma((2, 3)), dma((2, 3)),
             dma((2, 7)), dma((2, 7)), dma((2, 3)), dma((2, 3)),
         ],
         compiler_params=pltpu.CompilerParams(

time: 86.1 us -> 73.4 us (0.85)
  the two profiles are of different devices: /device:TPU:10 before, /device:TPU:0 now
where the time goes in v2:
time: 73.4 us; the launch traced here: 73.2 us
  Pallas kernels  72.5 us (99%)
    pallas_call x1, Pallas kernels, on_device_fast(): pl.pallas_call(functools.partial(exchange_kernel, entries), out_shape=(ja...  66.5 us
    pallas_call x1, Pallas kernels, on_device_fast(): pl.pallas_call(finish_kernel, grid=(n,), out_shape=tuple((jax.ShapeDtypeS...  5.97 us

profile of v2, /device:TPU:0, one launch (start us, length us, event | category | flops | bytes accessed | tf_op | source)
XLA Modules:
  0.0 73.2 jit_solution(17125580179333679840)
XLA Ops:
  0.6 66.5 %shard_map.161 = (bf16[2,4,128,512]{3,2,1,0:T(8,128)(2,1)}, f32[2,128,512]{2,1,0:T(8,128)}) custom-call(bf16[352,2048]{1,0:T(8,128)(2,1)} %si_hbm.1, bf16[352,2048]{1,0:T(8,128)(2,1)} %oc_hbm.1, bf16[352,512]{1,0:T(8,128)(2,1)} %qc_hbm.1, bf16[352,512]{1,0:T(8,128)(2,1)} %ao_hbm.1, bf16[512,512]{1,0:T(8,128)(2,1)} %qb.1, bf16[512,512]{1,0:T(8,128)(2,1)} %ob.1, ...), custom_call_target="tpu_custom_call" | custom-call | tf_op jit(solution)/shard_map/pallas_call | solution.py:390
  67.2 6.0 %shard_map.162 = (f32[512,512]{1,0:T(8,128)}, f32[512,512]{1,0:T(8,128)}, f32[512,512]{1,0:T(8,128)}, f32[512,512]{1,0:T(8,128)}, bf16[512,512]{1,0:T(8,128)(2,1...) custom-call(bf16[512,512]{1,0:T(8,128)(2,1)} %qb.1, bf16[512,512]{1,0:T(8,128)(2,1)} %ob.1, ...), custom_call_target="tpu_custom_call" | custom-call | flops 536870912 | bytes 5242880 | tf_op jit(solution)/shard_map/pallas_call | solution.py:436
